TPU v7x, 32 devices: a whole 2x2x4 slice. The times are simulated.
32 devices in a mesh: fs: 16 (over z, y, x), tp: 2 (over core).
Axes of the slice: x: 2, y: 2, z: 4, core: 2. Of those that a mesh axis runs over, the one named last changes fastest.
Arguments:
- inputs: bfloat16 [6144, 2048], P('fs'), may hold values from -6 to 6
- gain: float32 [2048], replicated, may hold values from 0.1 to 1.9
- w_gate: bfloat16 [2048, 2816], P('fs', 'tp'), may hold values from -0.125 to 0.125
- w_up: bfloat16 [2048, 2816], P('fs', 'tp'), may hold values from -0.125 to 0.125
- w_down: bfloat16 [2816, 2048], P('tp', 'fs'), may hold values from -0.109375 to 0.109375
- cotangent: bfloat16 [6144, 2048], P('fs'), may hold values from -6 to 6
Outputs:
- input_gradient: bfloat16 [6144, 2048], P('fs')
- grad_down: float32 [2816, 2048], P('tp', 'fs')
All inputs are finite; a program needn't handle non-finite values.
Results may differ from a plain program's by a relative error of at most 0.014.
Values may be sent and summed in bfloat16 or wider, within the bound.
A program may use at most 64 MiB of HBM per device.

v0:
```python
import jax
import jax.numpy as jnp
from jax import lax
from jax.sharding import PartitionSpec as P

EPSILON = 1e-06
HALF_STEP = 0.5


def contract_last(left, right):
    return lax.dot_general(
        left, right, (((1,), (1,)), ((), ())), preferred_element_type=jnp.float32
    )


def shards(inputs, gain, w_gate, w_up, w_down, cotangent):
    value_entries = inputs.astype(jnp.float32)
    inverse_norm_factor = lax.rsqrt(
        jnp.mean(value_entries * value_entries, axis=-1, keepdims=True) + EPSILON
    )
    normalized_input = value_entries * inverse_norm_factor
    normalized_rows = (normalized_input * gain).astype(jnp.bfloat16)
    whole_gate, whole_up = (
        lax.all_gather(w_gate, "fs", axis=0, tiled=True),
        lax.all_gather(w_up, "fs", axis=0, tiled=True),
    )
    gate_value = jnp.dot(normalized_rows, whole_gate, preferred_element_type=jnp.float32)
    up_projection_value = jnp.dot(normalized_rows, whole_up, preferred_element_type=jnp.float32)
    sigmoid_gate = jax.nn.sigmoid(gate_value)
    hidden = (gate_value * sigmoid_gate * up_projection_value).astype(jnp.bfloat16)
    d_hidden = HALF_STEP * contract_last(
        cotangent, lax.all_gather(w_down, "fs", axis=1, tiled=True)
    )
    down_term = HALF_STEP * lax.dot_general(
        hidden, cotangent, (((0,), (0,)), ((), ())), preferred_element_type=jnp.float32
    )
    grad_down = lax.psum_scatter(down_term, "fs", scatter_dimension=1, tiled=True)
    d_gate = (
        d_hidden * up_projection_value * sigmoid_gate * (1.0 + gate_value * (1.0 - sigmoid_gate))
    ).astype(jnp.bfloat16)
    d_up = (d_hidden * gate_value * sigmoid_gate).astype(jnp.bfloat16)
    partial_term = contract_last(d_gate, whole_gate) + contract_last(d_up, whole_up)
    d_normed = lax.psum(partial_term.astype(jnp.bfloat16), "tp").astype(jnp.float32)
    scaled_hidden = d_normed * gain
    input_gradient = inverse_norm_factor * (
        scaled_hidden
        - normalized_input * jnp.mean(scaled_hidden * normalized_input, axis=-1, keepdims=True)
    )
    return (input_gradient.astype(jnp.bfloat16), grad_down)


def solution(mesh):
    in_specs = (P("fs", None), P(), P("fs", "tp"), P("fs", "tp"), P("tp", "fs"), P("fs", None))
    out_specs = (P("fs", None), P("tp", "fs"))
    return jax.shard_map(shards, mesh=mesh, in_specs=in_specs, out_specs=out_specs, check_vma=False)
```

profile of v0, /device:TPU:10, one launch (start us, length us, event | category | flops | bytes accessed | tf_op | source)
XLA Modules:
  0.0 587.9 jit_solution(5369307967862374800)
XLA Ops:
  7.2 0.0 all-gather.8.cloned.1.call-start
  7.2 0.7 all-gather.8.cloned.1.call-update
  7.9 0.0 all-gather.6.cloned.1.call-start
  8.0 0.7 all-gather.6.cloned.1.call-update
  8.7 0.0 all-gather.4.cloned.1.call-start
  8.7 0.7 all-gather.4.cloned.1.call-update
  9.4 0.0 all-reduce.2.cloned.1.call-start
  9.5 1.8 fusion.8
  11.3 89.2 %all-gather.8.cloned.1.call-done = bf16[2048,1408]{1,0:T(8,128)(2,1)} async-done(((bf16[128,1408]{1,0:T(8,128)(2,1)}), bf16[2048,1408]{1,0:T(8,128)(2,1)}) %all-gather.8.cloned.1.call-update) | async-done | bytes 5767184 | tf_op jit(solution)/shard_map/all_gather | solution.py:24
  100.5 6.6 %fusion.13 = f32[384,1408]{1,0:T(8,128)} fusion(bf16[2048,1408]{1,0:T(8,128)(2,1)} %all-gather.8.cloned.1.call-done, bf16[384,2048]{1,0:T(8,128)(2,1)S(1)} %copy-done.1, f32[2048]{0:T(1024)S(1)} %copy-done.3, f32[384]{0:T(512)S(1)} %add_rsqrt_fusion), kind=kOutput, calls=%fused_computation.23 | convolution fusion | flops 2217738240 | bytes 9512448 | tf_op jit(solution)/shard_map/dot_general | solution.py:27
  107.1 83.5 %all-gather.6.cloned.1.call-done = bf16[2048,1408]{1,0:T(8,128)(2,1)} async-done(((bf16[128,1408]{1,0:T(8,128)(2,1)}), bf16[2048,1408]{1,0:T(8,128)(2,1)}) %all-gather.6.cloned.1.call-update) | async-done | bytes 5767184 | tf_op jit(solution)/shard_map/all_gather | solution.py:25
  190.6 6.7 %fusion.15 = f32[384,1408]{1,0:T(8,128)} fusion(bf16[2048,1408]{1,0:T(8,128)(2,1)} %all-gather.6.cloned.1.call-done, bf16[384,2048]{1,0:T(8,128)(2,1)S(1)} %copy-done.1, f32[2048]{0:T(1024)S(1)} %copy-done.3, f32[384]{0:T(512)S(1)} %add_rsqrt_fusion), kind=kOutput, calls=%fused_computation.24 | convolution fusion | flops 2217738240 | bytes 9512448 | tf_op jit(solution)/shard_map/dot_general | solution.py:28
  197.3 100.4 %all-gather.4.cloned.1.call-done = bf16[1408,2048]{1,0:T(8,128)(2,1)} async-done(((bf16[1408,128]{1,0:T(8,128)(2,1)}), bf16[1408,2048]{1,0:T(8,128)(2,1)}) %all-gather.4.cloned.1.call-update) | async-done | bytes 5767184 | tf_op jit(solution)/shard_map/all_gather | solution.py:32
  297.7 5.4 convolution_multiply_fusion.1
  303.2 0.1 copy-done.6
  303.3 3.2 fusion.9
  306.6 3.8 add_convert_fusion
  310.4 0.2 reduce-scatter.2.cloned.1.call-start
  310.6 8.5 %convolution_multiply_fusion = f32[1408,2048]{1,0:T(8,128)} fusion(bf16[384,2048]{1,0:T(8,128)(2,1)S(1)} %copy-done, f32[384,1408]{1,0:T(8,128)} %fusion.15, f32[384,1408]{1,0:T(8,128)} %fusion.13), kind=kOutput, calls=%fused_computation | convolution fusion | flops 2220720128 | bytes 17432576 | tf_op jit(solution)/shard_map/dot_general | solution.py:34
  319.1 0.0 reduce-scatter.2.cloned.1.call-update
  319.1 13.0 %all-reduce.2.cloned.1.call-done = bf16[384,2048]{1,0:T(8,128)(2,1)} async-done(((bf16[384,2048]{1,0:T(8,128)(2,1)}), bf16[384,2048]{1,0:T(8,128)(2,1)}) %all-reduce.2.cloned.1.call-update) | async-done | bytes 1572880 | tf_op jit(solution)/shard_map/psum | solution.py:43
  332.1 2.3 fusion.4
  334.4 2.0 fusion.7
  336.5 245.0 %reduce-scatter.2.cloned.1.call-done = f32[1408,128]{1,0:T(8,128)} async-done(((f32[1408,2048]{1,0:T(8,128)}), f32[1408,128]{1,0:T(8,128)}) %reduce-scatter.2.cloned.1.call-update) | async-done | bytes 720912 | tf_op jit(solution)/shard_map/reduce_scatter | solution.py:37
  (21 shorter events, 0.1 us)
Async XLA Ops:
  7.2 290.6 %copy-start = (bf16[384,2048]{1,0:T(8,128)(2,1)S(1)}, bf16[384,2048]{1,0:T(8,128)(2,1)}, u32[]{:S(2)}) copy-start(bf16[384,2048]{1,0:T(8,128)(2,1)} %param.11) | copy-start | bytes 4718596
  7.2 93.3 %copy-start.1 = (bf16[384,2048]{1,0:T(8,128)(2,1)S(1)}, bf16[384,2048]{1,0:T(8,128)(2,1)}, u32[]{:S(2)}) copy-start(bf16[384,2048]{1,0:T(8,128)(2,1)} %param.6) | copy-start | bytes 4718596
  7.2 93.3 %copy-start.3 = (f32[2048]{0:T(1024)S(1)}, f32[2048]{0:T(1024)}, u32[]{:S(2)}) copy-start(f32[2048]{0:T(1024)} %param.7) | copy-start | bytes 24580
  7.2 93.3 %all-gather.8.cloned.1.call-start = ((), (), s32[]{:S(2)}) async-start(), calls=%async_computation.3 | async-start | bytes 6127616 | tf_op jit(solution)/shard_map/all_gather | solution.py:24
  7.9 182.7 %all-gather.6.cloned.1.call-start = ((), (), s32[]{:S(2)}) async-start(), calls=%async_computation.2 | async-start | bytes 6127616 | tf_op jit(solution)/shard_map/all_gather | solution.py:25
  8.7 289.0 %all-gather.4.cloned.1.call-start = ((), (), s32[]{:S(2)}) async-start(), calls=%async_computation.1 | async-start | bytes 6127616 | tf_op jit(solution)/shard_map/all_gather | solution.py:32
  9.4 322.7 %all-reduce.2.cloned.1.call-start = ((), (), s32[]{:S(2)}) async-start(), calls=%async_computation.4 | async-start | bytes 3145728 | tf_op jit(solution)/shard_map/psum | solution.py:43
  297.7 5.4 copy-start.4
  297.7 5.5 copy-start.5
  297.7 5.6 copy-start.6
  297.7 8.8 %slice-start = ((s8[5767168]{0:T(1024)(128)(4,1)}), s8[4194304]{0:T(1024)(128)(4,1)S(1)}, s32[]{:S(2)}) async-start(s8[5767168]{0:T(1024)(128)(4,1)} %bitcast.7), calls=%async_computation.6 | async-start | bytes 8388608
  303.3 3.2 slice-start.1
  310.4 271.0 %reduce-scatter.2.cloned.1.call-start = ((), (), s32[]{:S(2)}) async-start(), calls=%async_computation.5 | async-start | bytes 12255232 | tf_op jit(solution)/shard_map/reduce_scatter | solution.py:37
  332.1 2.3 copy-start.2
Sparse Core Ops, SparseCore 0:
  10.7 89.7 all-gather.7
  103.2 87.4 all-gather.5
  193.3 104.3 all-gather.3
  310.5 21.5 all-reduce.1
  334.9 246.5 reduce-scatter.1
where the time goes:
time: 588 us
  waiting for transfers between devices  533 us (91%)
  matrix products  34.2 us (6%)
  between operations  13.9 us (2%)
  other arithmetic  6.11 us (1%)
    reduce_scatter x1, waiting for transfers between devices, shards(): lax.psum_scatter(down_term, 'fs', scatter_dimension=1, tiled=True)  245 us
    all_gather x1, waiting for transfers between devices, shards(): lax.all_gather(w_down, 'fs', axis=1, tiled=True)  100 us
    all_gather x1, waiting for transfers between devices, shards(): lax.all_gather(w_gate, 'fs', axis=0, tiled=True)  89.2 us
    all_gather x1, waiting for transfers between devices, shards(): lax.all_gather(w_up, 'fs', axis=0, tiled=True)  83.5 us
    psum x1, waiting for transfers between devices, shards(): lax.psum(partial_term.astype(jnp.bfloat16), 'tp').astype(jnp.float32)  13 us
    dot_general x3, matrix products, contract_last(): lax.dot_general(left, right, (((1,), (1,)), ((), ())), preferred_element_...  12.4 us
  transfers between devices with their start and end apart: 5, of which 5 were waited for; matrix products, arithmetic and copies ran while one was open for 5% of the time, Pallas kernels for 0%

commit v1 on v0

--- a/solution.py
+++ b/solution.py
@@ -28,9 +28,11 @@
     up_projection_value = jnp.dot(normalized_rows, whole_up, preferred_element_type=jnp.float32)
     sigmoid_gate = jax.nn.sigmoid(gate_value)
     hidden = (gate_value * sigmoid_gate * up_projection_value).astype(jnp.bfloat16)
-    d_hidden = HALF_STEP * contract_last(
-        cotangent, lax.all_gather(w_down, "fs", axis=1, tiled=True)
-    )
+
+    def obtain_target(vector):
+        return jnp.concatenate(lax.all_gather(vector, axis_name="fs"), 1)
+
+    d_hidden = HALF_STEP * contract_last(cotangent, obtain_target(w_down))
     down_term = HALF_STEP * lax.dot_general(
         hidden, cotangent, (((0,), (0,)), ((), ())), preferred_element_type=jnp.float32
     )

time: 588 us -> 569 us (0.968)
  waiting for transfers between devices: 533 us -> 505 us
  local copies, waits for them, and re-layouts: 0.19 us -> 8.63 us
    all_gather x1, waiting for transfers between devices: 89.2 us -> 75 us  [shards(): lax.all_gather(w_gate, 'fs', axis=0, tiled=True)]
    all_gather x1, waiting for transfers between devices: 100 us -> 89.2 us  [obtain_target(): return jnp.concatenate(lax.all_gather(vector, axis_name='fs'), 1)]
    reshape x0 -> x1, local copies, waits for them, and re-layouts: none -> 8.23 us  [obtain_target(): return jnp.concatenate(lax.all_gather(vector, axis_name='fs'), 1)]
  transfers between devices with their start and end apart: 5 -> 5, of which waited for: 5 -> 5; matrix products, arithmetic and copies ran while one was open for 5% -> 6% of each run, Pallas kernels for 0% -> 0%
where the time goes in v1:
time: 569 us
  waiting for transfers between devices  505 us (89%)
  matrix products  34.5 us (6%)
  between operations  13.8 us (2%)
  local copies, waits for them, and re-layouts  8.63 us (2%)
  other arithmetic  6.13 us (1%)
    reduce_scatter x1, waiting for transfers between devices, shards(): lax.psum_scatter(down_term, 'fs', scatter_dimension=1, tiled=True)  245 us
    all_gather x1, waiting for transfers between devices, obtain_target(): return jnp.concatenate(lax.all_gather(vector, axis_name='fs'), 1)  89.2 us
    all_gather x1, waiting for transfers between devices, shards(): lax.all_gather(w_up, 'fs', axis=0, tiled=True)  83.4 us
    all_gather x1, waiting for transfers between devices, shards(): lax.all_gather(w_gate, 'fs', axis=0, tiled=True)  75 us
    dot_general x3, matrix products, contract_last(): lax.dot_general(left, right, (((1,), (1,)), ((), ())), preferred_element_...  13.9 us
  transfers between devices with their start and end apart: 5, of which 5 were waited for; matrix products, arithmetic and copies ran while one was open for 6% of the time, Pallas kernels for 0%

profile of v1, /device:TPU:10, one launch (start us, length us, event | category | flops | bytes accessed | tf_op | source)
XLA Modules:
  0.0 569.0 jit_solution(7624442295028113220)
XLA Ops:
  7.2 0.7 all-gather.9.cloned.1.call-update
  7.9 0.0 all-gather.7.cloned.1.call-start
  8.0 0.7 all-gather.7.cloned.1.call-update
  8.7 0.0 all-gather.5.cloned.1.call-start
  8.7 0.7 all-gather.5.cloned.1.call-update
  9.4 0.0 all-reduce.2.cloned.1.call-start
  9.4 1.8 fusion.8
  11.2 89.2 %all-gather.9.cloned.1.call-done = bf16[22528,128]{1,0:T(8,128)(2,1)} async-done(((bf16[1408,128]{1,0:T(8,128)(2,1)}), bf16[22528,128]{1,0:T(8,128)(2,1)}) %all-gather.9.cloned.1.call-update) | async-done | bytes 5767184 | tf_op jit(solution)/shard_map/all_gather | solution.py:33
  100.5 8.2 %copy.8 = bf16[1408,16,128]{0,2,1:T(8,128)(2,1)} copy(bf16[1408,16,128]{2,0,1:T(8,128)(2,1)} %bitcast.11) | data formatting | bytes 11534336 | tf_op jit(solution)/shard_map/reshape | solution.py:33
  108.7 6.9 %convolution_multiply_fusion.1 = f32[384,1408]{1,0:T(8,128)} fusion(bf16[384,2048]{1,0:T(8,128)(2,1)S(1)} %copy-done, bf16[1408,2048]{0,1:T(8,128)(2,1)} %bitcast.12), kind=kOutput, calls=%fused_computation.14 | convolution fusion | flops 2215133184 | bytes 9502720 | tf_op jit(solution)/shard_map/dot_general | solution.py:11
  115.6 75.0 %all-gather.7.cloned.1.call-done = bf16[2048,1408]{1,0:T(8,128)(2,1)} async-done(((bf16[128,1408]{1,0:T(8,128)(2,1)}), bf16[2048,1408]{1,0:T(8,128)(2,1)}) %all-gather.7.cloned.1.call-update) | async-done | bytes 5767184 | tf_op jit(solution)/shard_map/all_gather | solution.py:24
  190.6 6.8 %fusion.13 = f32[384,1408]{1,0:T(8,128)} fusion(bf16[2048,1408]{1,0:T(8,128)(2,1)} %all-gather.7.cloned.1.call-done, bf16[384,2048]{1,0:T(8,128)(2,1)S(1)} %copy-done.1, f32[2048]{0:T(1024)S(1)} %copy-done.3, f32[384]{0:T(512)S(1)} %add_rsqrt_fusion), kind=kOutput, calls=%fused_computation.23 | convolution fusion | flops 2217738240 | bytes 9512448 | tf_op jit(solution)/shard_map/dot_general | solution.py:27
  197.4 83.4 %all-gather.5.cloned.1.call-done = bf16[2048,1408]{1,0:T(8,128)(2,1)} async-done(((bf16[128,1408]{1,0:T(8,128)(2,1)}), bf16[2048,1408]{1,0:T(8,128)(2,1)}) %all-gather.5.cloned.1.call-update) | async-done | bytes 5767184 | tf_op jit(solution)/shard_map/all_gather | solution.py:25
  280.8 5.4 fusion.15
  286.2 0.1 copy-done.8
  286.4 3.2 fusion.9
  289.6 0.2 copy-done.5
  289.8 3.8 add_convert_fusion
  293.6 0.2 reduce-scatter.2.cloned.1.call-start
  293.8 8.4 %convolution_multiply_fusion = f32[1408,2048]{1,0:T(8,128)} fusion(bf16[384,2048]{1,0:T(8,128)(2,1)S(1)} %copy-done, f32[384,1408]{1,0:T(8,128)} %copy-done.7, f32[384,1408]{1,0:T(8,128)} %fusion.13), kind=kOutput, calls=%fused_computation | convolution fusion | flops 2220720128 | bytes 17432576 | tf_op jit(solution)/shard_map/dot_general | solution.py:36
  302.3 10.9 %all-reduce.2.cloned.1.call-done = bf16[384,2048]{1,0:T(8,128)(2,1)} async-done(((bf16[384,2048]{1,0:T(8,128)(2,1)}), bf16[384,2048]{1,0:T(8,128)(2,1)}) %all-reduce.2.cloned.1.call-update) | async-done | bytes 1572880 | tf_op jit(solution)/shard_map/psum | solution.py:45
  313.2 2.3 fusion.4
  315.5 2.0 fusion.7
  317.5 244.9 %reduce-scatter.2.cloned.1.call-done = f32[1408,128]{1,0:T(8,128)} async-done(((f32[1408,2048]{1,0:T(8,128)}), f32[1408,128]{1,0:T(8,128)}) %reduce-scatter.2.cloned.1.call-update) | async-done | bytes 720912 | tf_op jit(solution)/shard_map/reduce_scatter | solution.py:39
  (21 shorter events, 0.1 us)
Async XLA Ops:
  7.2 101.5 %copy-start = (bf16[384,2048]{1,0:T(8,128)(2,1)S(1)}, bf16[384,2048]{1,0:T(8,128)(2,1)}, u32[]{:S(2)}) copy-start(bf16[384,2048]{1,0:T(8,128)(2,1)} %param.11) | copy-start | bytes 4718596
  7.2 93.3 %all-gather.9.cloned.1.call-start = ((), (), s32[]{:S(2)}) async-start(), calls=%async_computation.5 | async-start | bytes 6127616 | tf_op jit(solution)/shard_map/all_gather | solution.py:33
  7.9 182.7 %all-gather.7.cloned.1.call-start = ((), (), s32[]{:S(2)}) async-start(), calls=%async_computation.2 | async-start | bytes 6127616 | tf_op jit(solution)/shard_map/all_gather | solution.py:24
  8.7 272.1 %all-gather.5.cloned.1.call-start = ((), (), s32[]{:S(2)}) async-start(), calls=%async_computation.1 | async-start | bytes 6127616 | tf_op jit(solution)/shard_map/all_gather | solution.py:25
  9.4 303.8 %all-reduce.2.cloned.1.call-start = ((), (), s32[]{:S(2)}) async-start(), calls=%async_computation.3 | async-start | bytes 3145728 | tf_op jit(solution)/shard_map/psum | solution.py:45
  108.7 81.9 %copy-start.1 = (bf16[384,2048]{1,0:T(8,128)(2,1)S(1)}, bf16[384,2048]{1,0:T(8,128)(2,1)}, u32[]{:S(2)}) copy-start(bf16[384,2048]{1,0:T(8,128)(2,1)} %param.6) | copy-start | bytes 4718596
  108.7 81.9 %copy-start.3 = (f32[2048]{0:T(1024)S(1)}, f32[2048]{0:T(1024)}, u32[]{:S(2)}) copy-start(f32[2048]{0:T(1024)} %param.7) | copy-start | bytes 24580
  280.8 5.5 copy-start.4
  280.8 5.5 copy-start.6
  280.8 5.6 copy-start.8
  286.4 3.2 copy-start.7
  286.4 3.4 copy-start.5
  293.6 268.9 %reduce-scatter.2.cloned.1.call-start = ((), (), s32[]{:S(2)}) async-start(), calls=%async_computation.4 | async-start | bytes 12255232 | tf_op jit(solution)/shard_map/reduce_scatter | solution.py:39
  313.2 2.3 copy-start.2
Sparse Core Ops, SparseCore 0:
  10.7 89.7 all-gather.8
  103.2 87.4 all-gather.6
  193.3 87.4 all-gather.4
  293.7 19.4 all-reduce.1
  315.9 246.5 reduce-scatter.1
